TPU v7x, 512 devices: a whole 4x8x8 slice. The times are simulated.
512 devices in a mesh: rep: 64 (over z, y), fs: 4 (over x), tp: 2 (over core).
Axes of the slice: x: 4, y: 8, z: 8, core: 2. Of those that a mesh axis runs over, the one named last changes fastest.
Arguments:
- pre_act: bfloat16 [65536, 4096], P('rep', ('fs', 'tp')), may hold values from -6 to 6
- down_weight: bfloat16 [4096, 2048], P(('fs', 'tp')), may hold values from -0.09375 to 0.09375
- cotangent: bfloat16 [65536, 2048], P('rep', ('fs', 'tp')), may hold values from -16 to 16
Outputs:
- grad_pre: bfloat16 [65536, 4096], P('rep', ('fs', 'tp'))
- grad_weight: float32 [4096, 2048], P(('fs', 'tp', 'rep'))
All inputs are finite; a program needn't handle non-finite values.
Results may differ from a plain program's by a relative error of at most 0.0029.
Values may be sent and summed in bfloat16 or wider, within the bound.
No kernel may reach another device: no remote copies, remote signals or barrier semaphores. Data moves between devices by JAX's collectives and lax.ppermute only.
A program may use at most 64 MiB of HBM per device.

v0:
```python
import jax
import jax.numpy as jnp
from jax import lax
from jax.sharding import Mesh
from jax.sharding import PartitionSpec as P

REP = ("rep_0", "rep_1")
FS_TP_REP = ("fs", "tp", "rep_0", "rep_1")


def scatter_axes(shard, axes, dim):
    if not axes:
        return shard
    nearer = lax.psum_scatter(shard, axes[0], scatter_dimension=dim, tiled=True)
    return scatter_axes(nearer, axes[1:], dim)


def on_device(pre_act, down_weight, cotangent):
    whole = lax.all_gather(cotangent, ("fs", "tp"), axis=1, tiled=True)
    grad_hidden = lax.dot_general(
        whole, down_weight, (((1,), (1,)), ((), ())), preferred_element_type=jnp.float32
    )
    positive = jnp.maximum(pre_act.astype(jnp.float32), 0.0)
    grad_pre = (grad_hidden * 2.0 * positive).astype(jnp.bfloat16)
    hidden = (positive * positive).astype(jnp.bfloat16)
    factor = 1.0 / jnp.sqrt(jnp.float32(pre_act.shape[0] * lax.axis_size(REP)))
    term = lax.dot_general(
        hidden, whole, (((0,), (0,)), ((), ())), preferred_element_type=jnp.float32
    )
    summed = scatter_axes(term, REP, 0)
    return (grad_pre, summed * factor)


def solution(mesh):
    finer = Mesh(
        mesh.devices.reshape(8, 8, mesh.shape["fs"], mesh.shape["tp"]),
        ("rep_0", "rep_1", "fs", "tp"),
    )
    in_specs = (P(REP, ("fs", "tp")), P(("fs", "tp"), None), P(REP, ("fs", "tp")))
    out_specs = (P(REP, ("fs", "tp")), P(FS_TP_REP, None))
    return jax.shard_map(
        on_device, mesh=finer, in_specs=in_specs, out_specs=out_specs, check_vma=False
    )
```

profile of v0, /device:TPU:2, one launch (start us, length us, event | category | flops | bytes accessed | tf_op | source)
XLA Modules:
  0.0 171.4 jit_solution(6033609325006091810)
XLA Ops:
  7.2 0.0 copy-start
  7.2 0.0 all-gather.2.cloned.1.call-start
  7.2 0.7 all-gather.2.cloned.1.call-update
  7.9 0.0 reduce-scatter.3.cloned.1.call-start
  8.0 47.4 %all-gather.2.cloned.1.call-done = bf16[1024,2048]{1,0:T(8,128)(2,1)} async-done(((bf16[1024,256]{1,0:T(8,128)(2,1)}), bf16[1024,2048]{1,0:T(8,128)(2,1)}) %all-gather.2.cloned.1.call-update) | async-done | bytes 4194320 | tf_op jit(solution)/shard_map/all_gather | solution.py:19
  55.3 6.9 %fusion = f32[512,2048]{1,0:T(8,128)} fusion(bf16[1024,2048]{1,0:T(8,128)(2,1)} %all-gather.2.cloned.1.call-done, bf16[1024,512]{1,0:T(8,128)(2,1)} %param.3), kind=kOutput, calls=%fused_computation.3 | convolution fusion | flops 2149580800 | bytes 9437184 | tf_op jit(solution)/shard_map/dot_general | solution.py:27
  62.2 0.0 copy-start.1
  62.2 0.0 reduce-scatter.3.cloned.1.call-update
  62.2 0.0 reduce-scatter.5.cloned.1.call-start
  62.3 60.1 %reduce-scatter.3.cloned.1.call-done = f32[64,2048]{1,0:T(8,128)} async-done(((f32[512,2048]{1,0:T(8,128)}), f32[64,2048]{1,0:T(8,128)}) %reduce-scatter.3.cloned.1.call-update) | async-done | bytes 524304 | tf_op jit(solution)/shard_map/reduce_scatter | solution.py:14
  122.4 0.0 reduce-scatter.5.cloned.1.call-update
  122.4 0.0 copy-done
  122.4 0.0 copy-done.1
  122.4 5.5 %multiply_convert_fusion.1 = bf16[1024,512]{1,0:T(8,128)(2,1)} fusion(bf16[1024,512]{1,0:T(8,128)(2,1)S(1)} %copy-done.1, bf16[1024,2048]{1,0:T(8,128)(2,1)} %all-gather.2.cloned.1.call-done, bf16[512,2048]{1,0:T(8,128)(2,1)S(1)} %copy-done), kind=kOutput, calls=%fused_computation.1 | convolution fusion | flops 2150105088 | bytes 8388608 | tf_op jit(solution)/shard_map/dot_general | solution.py:20
  128.0 35.5 %reduce-scatter.5.cloned.1.call-done = f32[8,2048]{1,0:T(8,128)} async-done(((f32[64,2048]{1,0:T(8,128)}), f32[8,2048]{1,0:T(8,128)}) %reduce-scatter.5.cloned.1.call-update) | async-done | bytes 65552 | tf_op jit(solution)/shard_map/reduce_scatter | solution.py:14
  163.4 1.5 broadcast_multiply_fusion
Async XLA Ops:
  7.2 115.3 %copy-start = (bf16[512,2048]{1,0:T(8,128)(2,1)S(1)}, bf16[512,2048]{1,0:T(8,128)(2,1)}, u32[]{:S(2)}) copy-start(bf16[512,2048]{1,0:T(8,128)(2,1)} %param.4) | copy-start | bytes 6291460
  7.2 48.2 %all-gather.2.cloned.1.call-start = ((), (), s32[]{:S(2)}) async-start(), calls=%async_computation.2 | async-start | bytes 4718592 | tf_op jit(solution)/shard_map/all_gather | solution.py:19
  7.9 114.5 %reduce-scatter.3.cloned.1.call-start = ((), (), s32[]{:S(2)}) async-start(), calls=%async_computation.3 | async-start | bytes 4718592 | tf_op jit(solution)/shard_map/reduce_scatter | solution.py:14
  62.2 60.2 %copy-start.1 = (bf16[1024,512]{1,0:T(8,128)(2,1)S(1)}, bf16[1024,512]{1,0:T(8,128)(2,1)}, u32[]{:S(2)}) copy-start(bf16[1024,512]{1,0:T(8,128)(2,1)} %param.3) | copy-start | bytes 3145732
  62.2 101.2 %reduce-scatter.5.cloned.1.call-start = ((), (), s32[]{:S(2)}) async-start(), calls=%async_computation.4 | async-start | bytes 589824 | tf_op jit(solution)/shard_map/reduce_scatter | solution.py:14
Sparse Core Ops, SparseCore 0:
  10.1 45.1 all-gather.1
  62.4 60.0 reduce-scatter.2
  125.2 38.1 reduce-scatter.4
where the time goes:
time: 172 us; the launch traced here: 171 us
  waiting for transfers between devices  144 us (84%)
  between operations  13.8 us (8%)
  matrix products  12.4 us (7%)
    reduce_scatter x2, waiting for transfers between devices, scatter_axes(): nearer = lax.psum_scatter(shard, axes[0], scatter_dimension=dim, tiled=True)  95.6 us
    all_gather x1, waiting for transfers between devices, on_device(): whole = lax.all_gather(cotangent, ('fs', 'tp'), axis=1, tiled=True)  47.4 us
    dot_general x1, matrix products, on_device(): lax.dot_general(hidden, whole, (((0,), (0,)), ((), ())), preferred_elemen...  6.87 us
    dot_general x1, matrix products, on_device(): lax.dot_general(whole, down_weight, (((1,), (1,)), ((), ())), preferred_e...  5.53 us
  transfers between devices with their start and end apart: 3, of which 3 were waited for; matrix products, arithmetic and copies ran while one was open for 3% of the time, Pallas kernels for 0%

commit v1 on v0

v1 whole, which is shorter than its diff:
```python
import math

import jax
import jax.numpy as jnp
import numpy as np
from jax import lax
from jax.experimental import pallas as pl
from jax.experimental.pallas import tpu as pltpu
from jax.sharding import Mesh
from jax.sharding import PartitionSpec as P

REP = ("z", "y")
COL = ("fs", "tp")
GROUP = ("z", "y", "tp")
BF16 = jnp.bfloat16
F32 = jnp.float32


def lines(size):
    index = np.arange(size * size * 2).reshape(size, size, 2)
    return np.concatenate([index[..., 0].T, index[..., 1]]).tolist()


def other_lines(size):
    index = np.arange(size * size * 2).reshape(size, size, 2)
    return np.concatenate([index[..., 0], index[..., 1].T]).tolist()


def swap(rows, groups):
    parts = len(groups[0])
    got = lax.all_to_all(rows, GROUP, 0, 0, axis_index_groups=groups, tiled=True)
    return got.reshape(parts, rows.shape[0] // parts, rows.shape[1])


def other_core(x):
    return lax.ppermute(x, "tp", [(0, 1), (1, 0)])


def along(x, by):
    n = lax.axis_size("fs")
    pairs = [(2 * i + c, 2 * ((i + (by, -by)[c]) % n) + c) for i in range(n) for c in range(2)]
    return lax.ppermute(x, COL, pairs)


def piece(n, position):
    core = position % 2
    ahead = 2 * core - 1
    chip = (position // 2 + 4 + (0, 0, ahead, -ahead, -ahead, ahead, 2, 2)[n]) % 4
    return chip * 2 + (core + n) % 2


def hidden_kernel(at_ref, pre_ref, out_ref):
    units = pre_ref.shape[1]
    target = lax.broadcasted_iota(jnp.int32, (units, 1), 0)
    turned = target // 8 % 8 * 64 + target // 64 * 8 + target % 8
    source = jnp.where(at_ref[0] % 2 == 0, target, turned)
    pick = (lax.broadcasted_iota(jnp.int32, (units, units), 1) == source).astype(F32).astype(BF16)
    positive = jnp.maximum(pre_ref[...].astype(F32), 0.0)
    hidden = (positive * positive).astype(BF16)
    out_ref[...] = lax.dot_general(
        pick, hidden, (((1,), (1,)), ((), ())), preferred_element_type=F32
    ).astype(BF16)


def hidden_of(at, pre_act):
    tokens, units = pre_act.shape
    block = tokens // 2
    return pl.pallas_call(
        hidden_kernel,
        out_shape=jax.ShapeDtypeStruct((units, tokens), BF16),
        grid=(2,),
        in_specs=[
            pl.BlockSpec(memory_space=pltpu.SMEM),
            pl.BlockSpec((block, units), lambda i: (i, 0)),
        ],
        out_specs=pl.BlockSpec((units, block), lambda i: (0, i)),
        cost_estimate=pl.CostEstimate(
            flops=2 * units * units * tokens, bytes_accessed=4 * units * tokens, transcendentals=0
        ),
        name="hidden",
    )(at, pre_act)


def term_kernel(count, hidden_ref, *refs):
    out_ref = refs[-1]
    width = refs[0].shape[1]
    for n in range(count):
        out_ref[:, n * width : (n + 1) * width] = jnp.dot(
            hidden_ref[...], refs[n][...], preferred_element_type=F32
        ).astype(BF16)


def term_of(hidden, pieces, first, total, base=None):
    units, tokens = hidden.shape
    width = pieces[0].shape[1]
    count, steps = len(pieces), 2
    whole = pl.BlockSpec((tokens, width), lambda i: (0, 0))
    extra = () if base is None else (base,)
    return pl.pallas_call(
        lambda *refs: term_kernel(count, *refs),
        out_shape=jax.ShapeDtypeStruct((units, width * total), BF16),
        grid=(steps,),
        in_specs=[pl.BlockSpec((units // steps, tokens), lambda i: (i, 0))]
        + [whole] * count
        + [pl.BlockSpec(memory_space=pl.ANY)] * len(extra),
        out_specs=pl.BlockSpec((units // steps, width * count), lambda i: (i, first // count)),
        input_output_aliases={1 + count: 0} if extra else {},
        cost_estimate=pl.CostEstimate(
            flops=2 * units * tokens * width * count,
            bytes_accessed=2 * (units * tokens + width * count * (tokens + units)),
            transcendentals=0,
        ),
        name="term",
    )(hidden, *pieces, *extra)


def grad_pre_kernel(at_ref, pre_ref, weight_ref, *refs):
    parts, out_ref = refs[:-1], refs[-1]
    width = parts[0].shape[1]
    total = jnp.zeros(out_ref.shape, F32)
    for n, part in enumerate(parts):
        columns = pl.ds(pl.multiple_of(piece(n, at_ref[0]) * width, width), width)
        total += lax.dot_general(
            part[...], weight_ref[:, columns], (((1,), (1,)), ((), ())), preferred_element_type=F32
        )
    positive = jnp.maximum(pre_ref[...].astype(F32), 0.0)
    out_ref[...] = (total * 2.0 * positive).astype(BF16)


def grad_pre_of(at, pre_act, down_weight, parts):
    tokens, units = pre_act.shape
    block = tokens // 4
    width = parts[0].shape[1]
    return pl.pallas_call(
        grad_pre_kernel,
        out_shape=jax.ShapeDtypeStruct((tokens, units), BF16),
        grid=(4,),
        in_specs=[
            pl.BlockSpec(memory_space=pltpu.SMEM),
            pl.BlockSpec((block, units), lambda i: (i, 0)),
            pl.BlockSpec(down_weight.shape, lambda i: (0, 0)),
        ]
        + [pl.BlockSpec((block, width), lambda i: (i, 0))] * len(parts),
        out_specs=pl.BlockSpec((block, units), lambda i: (i, 0)),
        cost_estimate=pl.CostEstimate(
            flops=2 * tokens * units * width * len(parts),
            bytes_accessed=2 * (2 * tokens * units + down_weight.size + tokens * width * len(parts)),
            transcendentals=0,
        ),
        name="grad_pre",
    )(at, pre_act, down_weight, *parts)


def place_kernel(factor, width, at_ref, got_ref, out_ref):
    for n in range(out_ref.shape[1] // width):
        columns = slice(n * width, (n + 1) * width)
        total = got_ref[0, :, columns].astype(F32)
        for k in range(1, got_ref.shape[0]):
            total += got_ref[k, :, columns].astype(F32)
        target = pl.ds(pl.multiple_of(piece(n, at_ref[0]) * width, width), width)
        out_ref[:, target] = total * factor


def place(at, got, factor, width):
    return pl.pallas_call(
        lambda *refs: place_kernel(factor, width, *refs),
        out_shape=jax.ShapeDtypeStruct(got.shape[1:], F32),
        in_specs=[
            pl.BlockSpec(memory_space=pltpu.SMEM),
            pl.BlockSpec(memory_space=pltpu.VMEM),
        ],
        out_specs=pl.BlockSpec(memory_space=pltpu.VMEM),
        cost_estimate=pl.CostEstimate(
            flops=got.size, bytes_accessed=4 * got.size, transcendentals=0
        ),
        name="place",
    )(at, got)


def step(pre_act, down_weight, cotangent):
    tokens, width = cotangent.shape
    size = lax.axis_size("z")
    at = lax.axis_index(COL).astype(jnp.int32).reshape(1)

    one = along(cotangent, 1)
    own = other_core(cotangent)
    two = along(cotangent, -1)
    three = along(one, 1)
    pieces = (cotangent, own, one, other_core(one))
    pieces += (two, other_core(two), three, other_core(three))

    hidden = hidden_of(at, pre_act)
    term = term_of(hidden, pieces[:6], 0, 8)
    term = term_of(hidden, pieces[6:], 6, 8, term)
    got = swap(term, lines(size))
    joined = jnp.sum(got.astype(F32), axis=0).astype(BF16)
    got = swap(joined, other_lines(size))

    factor = 1.0 / math.sqrt(tokens * size * size)
    grad_weight = place(at, got, factor, width)
    grad_pre = grad_pre_of(at, pre_act, down_weight, pieces)
    return (grad_pre, grad_weight)


def solution(mesh):
    finer = Mesh(
        mesh.devices.reshape(8, 8, mesh.shape["fs"], mesh.shape["tp"]),
        REP + COL,
    )
    in_specs = (P(REP, COL), P(COL, None), P(REP, COL))
    out_specs = (P(REP, COL), P(COL + REP, None))
    return jax.shard_map(step, mesh=finer, in_specs=in_specs, out_specs=out_specs, check_vma=False)
```

time: 172 us -> 104 us (0.60)
  the two profiles are of different devices: /device:TPU:2 before, /device:TPU:4 now
where the time goes in v1:
time: 104 us
  blocking collectives  38.8 us (37%)
  starting transfers between devices  26.6 us (26%)
  Pallas kernels  19.3 us (19%)
  waiting for transfers between devices  14.5 us (14%)
  local copies, waits for them, and re-layouts  2.45 us (2%)
  other arithmetic  1.09 us (1%)
    all_to_all x1, blocking collectives, swap(): lax.all_to_all(rows, GROUP, 0, 0, axis_index_groups=groups, tiled=True)  38.8 us
    ppermute x3, starting transfers between devices, along(): return lax.ppermute(x, COL, pairs)  11.3 us
    ppermute x3, waiting for transfers between devices, along(): return lax.ppermute(x, COL, pairs)  10.9 us
    ppermute x4, starting transfers between devices, other_core(): return lax.ppermute(x, 'tp', [(0, 1), (1, 0)])  8.16 us
    pallas_call x2, Pallas kernels, term_of(): pl.pallas_call(lambda *refs: term_kernel(count, *refs), out_shape=jax.Sha...  7.92 us
    all_to_all x1, starting transfers between devices, swap(): lax.all_to_all(rows, GROUP, 0, 0, axis_index_groups=groups, tiled=True)  7.1 us
    pallas_call x1, Pallas kernels, grad_pre_of(): pl.pallas_call(grad_pre_kernel, out_shape=jax.ShapeDtypeStruct((tokens, u...  6.87 us
    all_to_all x1, waiting for transfers between devices, swap(): lax.all_to_all(rows, GROUP, 0, 0, axis_index_groups=groups, tiled=True)  3.62 us
  transfers between devices with their start and end apart: 8, of which 3 were waited for; matrix products, arithmetic and copies ran while one was open for 0% of the time, Pallas kernels for 14%

profile of v1, /device:TPU:4, one launch (start us, length us, event | category | flops | bytes accessed | tf_op | source)
XLA Modules:
  0.0 103.5 jit_solution(5793953955224002671)
XLA Ops:
  0.6 3.1 %collective-permute-start.1 = (bf16[1024,256]{1,0:T(8,128)(2,1)}, bf16[1024,256]{1,0:T(8,128)(2,1)S(1)}, u32[]{:S(2)}, u32[]{:S(2)}) collective-permute-start(bf16[1024,256]{1,0:T(8,128)(2,1)} %refs_1_.1), channel_id=1, source_target_pairs={{0,2},{1,7},{2,4},{3,1},{4,6},{5,3},{6,0},{7,5},{8,10},{9,15},{10,... | collective-permute-start | bytes 1572872 | tf_op jit(solution)/shard_map/ppermute | solution.py:42
  3.7 2.7 %collective-permute-start.3 = (bf16[1024,256]{1,0:T(8,128)(2,1)}, bf16[1024,256]{1,0:T(8,128)(2,1)S(1)}, u32[]{:S(2)}, u32[]{:S(2)}) collective-permute-start(bf16[1024,256]{1,0:T(8,128)(2,1)} %refs_1_.1), channel_id=1, source_target_pairs={{0,6},{1,3},{2,0},{3,5},{4,2},{5,7},{6,4},{7,1},{8,14},{9,11},{10,... | collective-permute-start | bytes 1572872 | tf_op jit(solution)/shard_map/ppermute | solution.py:42
  6.5 10.0 %collective-permute-done.1.refs_2_.refs_3_ = bf16[1024,256]{1,0:T(8,128)(2,1)S(1)} collective-permute-done((bf16[1024,256]{1,0:T(8,128)(2,1)}, bf16[1024,256]{1,0:T(8,128)(2,1)S(1)}, u32[]{:S(2)}, u32[]{:S(2)}) %collective-permute-start.1) | collective-permute-done | bytes 524320 | tf_op jit(solution)/shard_map/ppermute | solution.py:42
  16.5 5.5 %collective-permute-start.5 = (bf16[1024,256]{1,0:T(8,128)(2,1)S(1)}, bf16[1024,256]{1,0:T(8,128)(2,1)S(1)}, u32[]{:S(2)}, u32[]{:S(2)}) collective-permute-start(bf16[1024,256]{1,0:T(8,128)(2,1)S(1)} %collective-permute-done.1.refs_2_.refs_3_), channel_id=1, source_target_pairs={{0,2},{1,7},{2,4},{3,1},{4,6},{5,3},{6,0},{7,5},{8,10},{9,15},{10,... | collective-permute-start | bytes 1572872 | tf_op jit(solution)/shard_map/ppermute | solution.py:42
  22.0 1.9 %collective-permute-start = (bf16[1024,256]{1,0:T(8,128)(2,1)}, bf16[1024,256]{1,0:T(8,128)(2,1)S(1)}, u32[]{:S(2)}, u32[]{:S(2)}) collective-permute-start(bf16[1024,256]{1,0:T(8,128)(2,1)} %refs_1_.1), channel_id=1, source_target_pairs={{0,1},{1,0},{2,3},{3,2},{4,5},{5,4},{6,7},{7,6},{8,9},{9,8},{10,11... | collective-permute-start | bytes 1572872 | tf_op jit(solution)/shard_map/ppermute | solution.py:36
  23.9 0.0 collective-permute-done.3.refs_4_.refs_5_
  23.9 0.0 copy-start.1
  24.0 2.4 %collective-permute-start.4 = (bf16[1024,256]{1,0:T(8,128)(2,1)S(1)}, bf16[1024,256]{1,0:T(8,128)(2,1)S(1)}, u32[]{:S(2)}, u32[]{:S(2)}) collective-permute-start(bf16[1024,256]{1,0:T(8,128)(2,1)S(1)} %collective-permute-done.3.refs_4_.refs_5_), channel_id=1, source_target_pairs={{0,1},{1,0},{2,3},{3,2},{4,5},{5,4},{6,7},{7,6},{8,9},{9,8},{10,11... | collective-permute-start | bytes 1572872 | tf_op jit(solution)/shard_map/ppermute | solution.py:36
  26.4 1.9 %collective-permute-start.2 = (bf16[1024,256]{1,0:T(8,128)(2,1)S(1)}, bf16[1024,256]{1,0:T(8,128)(2,1)S(1)}, u32[]{:S(2)}, u32[]{:S(2)}) collective-permute-start(bf16[1024,256]{1,0:T(8,128)(2,1)S(1)} %collective-permute-done.1.refs_2_.refs_3_), channel_id=1, source_target_pairs={{0,1},{1,0},{2,3},{3,2},{4,5},{5,4},{6,7},{7,6},{8,9},{9,8},{10,11... | collective-permute-start | bytes 1572872 | tf_op jit(solution)/shard_map/ppermute | solution.py:36
  28.3 0.9 collective-permute-done.5.refs_6_.refs_1_
  29.2 1.9 %collective-permute-start.6 = (bf16[1024,256]{1,0:T(8,128)(2,1)S(1)}, bf16[1024,256]{1,0:T(8,128)(2,1)}, u32[]{:S(2)}, u32[]{:S(2)}) collective-permute-start(bf16[1024,256]{1,0:T(8,128)(2,1)S(1)} %collective-permute-done.5.refs_6_.refs_1_), channel_id=1, source_target_pairs={{0,1},{1,0},{2,3},{3,2},{4,5},{5,4},{6,7},{7,6},{8,9},{9,8},{10,11... | collective-permute-start | bytes 1572872 | tf_op jit(solution)/shard_map/ppermute | solution.py:36
  31.1 2.9 %hidden.1.refs_0_ = bf16[512,1024]{1,0:T(8,128)(2,1)} custom-call(s32[1]{0:T(128)} %bitcast.at_ref.refs_0_, bf16[1024,512]{1,0:T(8,128)(2,1)} %pre_ref.3), custom_call_target="tpu_custom_call" | custom-call | flops 536870912 | bytes 2097152 | tf_op jit(solution)/shard_map/hidden/pallas_call | solution.py:68
  34.0 0.0 collective-permute-done.refs_1_.refs_2_
  34.0 0.0 collective-permute-done.4.refs_5_.refs_6_
  34.0 0.0 copy-start.4
  34.0 0.0 collective-permute-done.2.refs_3_.refs_4_
  34.0 0.0 copy-done
  34.0 0.0 copy-done.1
  34.0 0.7 copy-done.3
  34.8 0.2 copy-done.4
  35.0 0.8 copy-done.5
  35.8 4.9 %term.2.refs_3_ = bf16[512,2048]{1,0:T(8,128)(2,1)} custom-call(bf16[512,1024]{1,0:T(8,128)(2,1)} %hidden.1.refs_0_, bf16[1024,256]{1,0:T(8,128)(2,1)} %refs_1_.1, bf16[1024,256]{1,0:T(8,128)(2,1)} %copy-done.3, bf16[1024,256]{1,0:T(8,128)(2,1)} %copy-done, bf16[1024,256]{1,0:T(8,128)(2,1)} %copy-done.5, bf16[1024,256]{1,0:T(8,128)(2,1)} %copy-done.1, ...), custom_call_target="tpu_custom_call" | custom-call | flops 1610612736 | bytes 5767168 | tf_op jit(solution)/shard_map/term/pallas_call | solution.py:99
  40.7 0.0 copy-done.2
  40.7 0.0 collective-permute-done.6.refs_7_.refs_2_
  40.7 3.0 %term.3 = bf16[512,2048]{1,0:T(8,128)(2,1)} custom-call(bf16[512,1024]{1,0:T(8,128)(2,1)} %hidden.1.refs_0_, bf16[1024,256]{1,0:T(8,128)(2,1)} %copy-done.2, bf16[1024,256]{1,0:T(8,128)(2,1)} %collective-permute-done.6.refs_7_.refs_2_, bf16[512,2048]{1,0:T(8,128)(2,1)} %term.2.refs_3_), custom_call_target="tpu_custom_call", output_to_operand_aliasing={{}: (3, {})} | custom-call | flops 536870912 | bytes 2621440 | tf_op jit(solution)/shard_map/term/pallas_call | solution.py:99
  43.7 38.8 %all_to_all.18 = bf16[8,64,2048]{2,1,0:T(8,128)(2,1)S(1)} all-to-all(bf16[8,64,2048]{2,1,0:T(8,128)(2,1)} %bitcast.3), channel_id=1, replica_groups={{0,64,128,192,256,320,384,448},{8,72,136,200,264,328,392,456},{16,80,14..., dimensions={0} | all-to-all | bytes 4194304 | tf_op jit(solution)/shard_map/all_to_all | solution.py:31
  82.5 1.1 %reduce_sum.12 = bf16[64,2048]{1,0:T(8,128)(2,1)} reduce(bf16[8,64,2048]{2,1,0:T(8,128)(2,1)S(1)} %all_to_all.18, bf16[]{:T(256)} %constant.12.clone.1), dimensions={0}, to_apply=%region_0.0 | reduce | flops 917504 | bytes 2359298 | tf_op jit(solution)/shard_map/reduce_sum | solution.py:196
  83.6 7.1 %all-to-all-start.1 = ((bf16[8,8,2048]{2,1,0:T(8,128)(2,1)}), bf16[8,8,2048]{2,1,0:T(8,128)(2,1)S(1)}, u32[]{:S(2)}, u32[]{:S(2)}) async-start(bf16[8,8,2048]{2,1,0:T(8,128)(2,1)} %bitcast.2), calls=%async_computation.1 | async-start | bytes 524288 | tf_op jit(solution)/shard_map/all_to_all | solution.py:31
  90.7 6.9 %grad_pre.1 = bf16[1024,512]{1,0:T(8,128)(2,1)} custom-call(s32[1]{0:T(128)} %bitcast.at_ref.refs_0_, bf16[1024,512]{1,0:T(8,128)(2,1)} %pre_ref.3, bf16[512,2048]{1,0:T(8,128)(2,1)} %weight_ref.1, bf16[1024,256]{1,0:T(8,128)(2,1)} %refs_1_.1, bf16[1024,256]{1,0:T(8,128)(2,1)} %copy-done.3, bf16[1024,256]{1,0:T(8,128)(2,1)} %copy-done, ...), custom_call_target="tpu_custom_call" | custom-call | flops 2147483648 | bytes 8388608 | tf_op jit(solution)/shard_map/grad_pre/pallas_call | solution.py:134
  97.6 3.6 %all-to-all-done.1.refs_1_ = bf16[8,8,2048]{2,1,0:T(8,128)(2,1)S(1)} async-done(((bf16[8,8,2048]{2,1,0:T(8,128)(2,1)}), bf16[8,8,2048]{2,1,0:T(8,128)(2,1)S(1)}, u32[]{:S(2)}, u32[]{:S(2)}) %all-to-all-start.1) | async-done | bytes 262176 | tf_op jit(solution)/shard_map/all_to_all | solution.py:31
  101.2 0.7 copy-done.6
  101.9 1.6 %place.1 = f32[8,2048]{1,0:T(8,128)} custom-call(s32[1]{0:T(128)} %bitcast.at_ref.refs_0_, bf16[8,8,2048]{2,1,0:T(8,128)(2,1)} %copy-done.6), custom_call_target="tpu_custom_call" | custom-call | flops 131072 | bytes 524288 | tf_op jit(solution)/shard_map/place/pallas_call | solution.py:165
  (5 shorter events, 0.0 us)
Async XLA Ops:
  0.6 15.9 %collective-permute-start.1 = (bf16[1024,256]{1,0:T(8,128)(2,1)}, bf16[1024,256]{1,0:T(8,128)(2,1)S(1)}, u32[]{:S(2)}, u32[]{:S(2)}) collective-permute-start(bf16[1024,256]{1,0:T(8,128)(2,1)} %refs_1_.1), channel_id=1, source_target_pairs={{0,2},{1,7},{2,4},{3,1},{4,6},{5,3},{6,0},{7,5},{8,10},{9,15},{10,... | collective-permute-start | bytes 1572872 | tf_op jit(solution)/shard_map/ppermute | solution.py:42
  3.7 20.2 %collective-permute-start.3 = (bf16[1024,256]{1,0:T(8,128)(2,1)}, bf16[1024,256]{1,0:T(8,128)(2,1)S(1)}, u32[]{:S(2)}, u32[]{:S(2)}) collective-permute-start(bf16[1024,256]{1,0:T(8,128)(2,1)} %refs_1_.1), channel_id=1, source_target_pairs={{0,6},{1,3},{2,0},{3,5},{4,2},{5,7},{6,4},{7,1},{8,14},{9,11},{10,... | collective-permute-start | bytes 1572872 | tf_op jit(solution)/shard_map/ppermute | solution.py:42
  16.5 17.5 %copy-start = (bf16[1024,256]{1,0:T(8,128)(2,1)}, bf16[1024,256]{1,0:T(8,128)(2,1)S(1)}, u32[]{:S(2)}) copy-start(bf16[1024,256]{1,0:T(8,128)(2,1)S(1)} %collective-permute-done.1.refs_2_.refs_3_) | copy-start | bytes 1572868
  16.5 12.7 %collective-permute-start.5 = (bf16[1024,256]{1,0:T(8,128)(2,1)S(1)}, bf16[1024,256]{1,0:T(8,128)(2,1)S(1)}, u32[]{:S(2)}, u32[]{:S(2)}) collective-permute-start(bf16[1024,256]{1,0:T(8,128)(2,1)S(1)} %collective-permute-done.1.refs_2_.refs_3_), channel_id=1, source_target_pairs={{0,2},{1,7},{2,4},{3,1},{4,6},{5,3},{6,0},{7,5},{8,10},{9,15},{10,... | collective-permute-start | bytes 1572872 | tf_op jit(solution)/shard_map/ppermute | solution.py:42
  22.0 12.0 %collective-permute-start = (bf16[1024,256]{1,0:T(8,128)(2,1)}, bf16[1024,256]{1,0:T(8,128)(2,1)S(1)}, u32[]{:S(2)}, u32[]{:S(2)}) collective-permute-start(bf16[1024,256]{1,0:T(8,128)(2,1)} %refs_1_.1), channel_id=1, source_target_pairs={{0,1},{1,0},{2,3},{3,2},{4,5},{5,4},{6,7},{7,6},{8,9},{9,8},{10,11... | collective-permute-start | bytes 1572872 | tf_op jit(solution)/shard_map/ppermute | solution.py:36
  23.9 10.1 %copy-start.1 = (bf16[1024,256]{1,0:T(8,128)(2,1)}, bf16[1024,256]{1,0:T(8,128)(2,1)S(1)}, u32[]{:S(2)}) copy-start(bf16[1024,256]{1,0:T(8,128)(2,1)S(1)} %collective-permute-done.3.refs_4_.refs_5_) | copy-start | bytes 1572868
  24.0 10.1 %collective-permute-start.4 = (bf16[1024,256]{1,0:T(8,128)(2,1)S(1)}, bf16[1024,256]{1,0:T(8,128)(2,1)S(1)}, u32[]{:S(2)}, u32[]{:S(2)}) collective-permute-start(bf16[1024,256]{1,0:T(8,128)(2,1)S(1)} %collective-permute-done.3.refs_4_.refs_5_), channel_id=1, source_target_pairs={{0,1},{1,0},{2,3},{3,2},{4,5},{5,4},{6,7},{7,6},{8,9},{9,8},{10,11... | collective-permute-start | bytes 1572872 | tf_op jit(solution)/shard_map/ppermute | solution.py:36
  26.4 7.7 %collective-permute-start.2 = (bf16[1024,256]{1,0:T(8,128)(2,1)S(1)}, bf16[1024,256]{1,0:T(8,128)(2,1)S(1)}, u32[]{:S(2)}, u32[]{:S(2)}) collective-permute-start(bf16[1024,256]{1,0:T(8,128)(2,1)S(1)} %collective-permute-done.1.refs_2_.refs_3_), channel_id=1, source_target_pairs={{0,1},{1,0},{2,3},{3,2},{4,5},{5,4},{6,7},{7,6},{8,9},{9,8},{10,11... | collective-permute-start | bytes 1572872 | tf_op jit(solution)/shard_map/ppermute | solution.py:36
  29.2 11.5 %copy-start.2 = (bf16[1024,256]{1,0:T(8,128)(2,1)}, bf16[1024,256]{1,0:T(8,128)(2,1)S(1)}, u32[]{:S(2)}) copy-start(bf16[1024,256]{1,0:T(8,128)(2,1)S(1)} %collective-permute-done.5.refs_6_.refs_1_) | copy-start | bytes 1572868
  29.2 11.5 %collective-permute-start.6 = (bf16[1024,256]{1,0:T(8,128)(2,1)S(1)}, bf16[1024,256]{1,0:T(8,128)(2,1)}, u32[]{:S(2)}, u32[]{:S(2)}) collective-permute-start(bf16[1024,256]{1,0:T(8,128)(2,1)S(1)} %collective-permute-done.5.refs_6_.refs_1_), channel_id=1, source_target_pairs={{0,1},{1,0},{2,3},{3,2},{4,5},{5,4},{6,7},{7,6},{8,9},{9,8},{10,11... | collective-permute-start | bytes 1572872 | tf_op jit(solution)/shard_map/ppermute | solution.py:36
  34.0 0.8 copy-start.3
  34.0 1.0 copy-start.4
  35.0 0.8 copy-start.5
  83.6 17.6 %all-to-all-start.1 = ((bf16[8,8,2048]{2,1,0:T(8,128)(2,1)}), bf16[8,8,2048]{2,1,0:T(8,128)(2,1)S(1)}, u32[]{:S(2)}, u32[]{:S(2)}) async-start(bf16[8,8,2048]{2,1,0:T(8,128)(2,1)} %bitcast.2), calls=%async_computation.1 | async-start | bytes 524288 | tf_op jit(solution)/shard_map/all_to_all | solution.py:31
  101.2 0.7 copy-start.6

commit v2 on v1

--- a/solution.py
+++ b/solution.py
@@ -14,6 +14,8 @@
 GROUP = ("z", "y", "tp")
 BF16 = jnp.bfloat16
 F32 = jnp.float32
+VMEM = pl.BlockSpec(memory_space=pltpu.VMEM)
+SMALL = pltpu.CompilerParams(vmem_limit_bytes=16 * 2**20)
 
 
 def lines(size):
@@ -77,6 +79,7 @@
         cost_estimate=pl.CostEstimate(
             flops=2 * units * units * tokens, bytes_accessed=4 * units * tokens, transcendentals=0
         ),
+        compiler_params=SMALL,
         name="hidden",
     )(at, pre_act)
 
@@ -93,18 +96,16 @@
 def term_of(hidden, pieces, first, total, base=None):
     units, tokens = hidden.shape
     width = pieces[0].shape[1]
-    count, steps = len(pieces), 2
-    whole = pl.BlockSpec((tokens, width), lambda i: (0, 0))
+    count = len(pieces)
     extra = () if base is None else (base,)
     return pl.pallas_call(
         lambda *refs: term_kernel(count, *refs),
         out_shape=jax.ShapeDtypeStruct((units, width * total), BF16),
-        grid=(steps,),
-        in_specs=[pl.BlockSpec((units // steps, tokens), lambda i: (i, 0))]
-        + [whole] * count
-        + [pl.BlockSpec(memory_space=pl.ANY)] * len(extra),
-        out_specs=pl.BlockSpec((units // steps, width * count), lambda i: (i, first // count)),
+        grid=(1,),
+        in_specs=[VMEM] * (1 + count) + [pl.BlockSpec(memory_space=pl.ANY)] * len(extra),
+        out_specs=pl.BlockSpec((units, width * count), lambda i: (0, first // count)),
         input_output_aliases={1 + count: 0} if extra else {},
+        compiler_params=SMALL,
         cost_estimate=pl.CostEstimate(
             flops=2 * units * tokens * width * count,
             bytes_accessed=2 * (units * tokens + width * count * (tokens + units)),
@@ -173,6 +174,7 @@
         cost_estimate=pl.CostEstimate(
             flops=got.size, bytes_accessed=4 * got.size, transcendentals=0
         ),
+        compiler_params=SMALL,
         name="place",
     )(at, got)
 
@@ -190,8 +192,8 @@
     pieces += (two, other_core(two), three, other_core(three))
 
     hidden = hidden_of(at, pre_act)
-    term = term_of(hidden, pieces[:6], 0, 8)
-    term = term_of(hidden, pieces[6:], 6, 8, term)
+    term = term_of(hidden, pieces[:4], 0, 8)
+    term = term_of(hidden, pieces[4:], 4, 8, term)
     got = swap(term, lines(size))
     joined = jnp.sum(got.astype(F32), axis=0).astype(BF16)
     got = swap(joined, other_lines(size))

time: 104 us -> 95.9 us (0.922)
  Pallas kernels: 19.3 us -> 12.3 us
  local copies, waits for them, and re-layouts: 2.45 us -> 1.24 us
    pallas_call x2, Pallas kernels: 7.92 us -> 3.7 us  [term_of(): pl.pallas_call(lambda *refs: term_kernel(count, *refs), out_shape=jax.Sha...]
    pallas_call x1, Pallas kernels: 2.89 us -> 1.1 us  [hidden_of(): pl.pallas_call(hidden_kernel, out_shape=jax.ShapeDtypeStruct((units, toke...]
    unnamed x14, local copies, waits for them, and re-layouts: 2.45 us -> 1.24 us
  transfers between devices with their start and end apart: 8 -> 8, of which waited for: 3 -> 3; matrix products, arithmetic and copies ran while one was open for 0% -> 0% of each run, Pallas kernels for 14% -> 11%
where the time goes in v2:
time: 95.9 us; the launch traced here: 95.3 us
  blocking collectives  38.6 us (40%)
  starting transfers between devices  26.6 us (28%)
  waiting for transfers between devices  14.5 us (15%)
  Pallas kernels  12.3 us (13%)
  local copies, waits for them, and re-layouts  1.24 us (1%)
  other arithmetic  1.11 us (1%)
    all_to_all x1, blocking collectives, swap(): lax.all_to_all(rows, GROUP, 0, 0, axis_index_groups=groups, tiled=True)  38.6 us
    ppermute x3, starting transfers between devices, along(): return lax.ppermute(x, COL, pairs)  11.3 us
    ppermute x3, waiting for transfers between devices, along(): return lax.ppermute(x, COL, pairs)  10.9 us
    ppermute x4, starting transfers between devices, other_core(): return lax.ppermute(x, 'tp', [(0, 1), (1, 0)])  8.16 us
    all_to_all x1, starting transfers between devices, swap(): lax.all_to_all(rows, GROUP, 0, 0, axis_index_groups=groups, tiled=True)  7.1 us
    pallas_call x1, Pallas kernels, grad_pre_of(): pl.pallas_call(grad_pre_kernel, out_shape=jax.ShapeDtypeStruct((tokens, u...  6.86 us
    pallas_call x2, Pallas kernels, term_of(): pl.pallas_call(lambda *refs: term_kernel(count, *refs), out_shape=jax.Sha...  3.7 us
    all_to_all x1, waiting for transfers between devices, swap(): lax.all_to_all(rows, GROUP, 0, 0, axis_index_groups=groups, tiled=True)  3.62 us
  transfers between devices with their start and end apart: 8, of which 3 were waited for; matrix products, arithmetic and copies ran while one was open for 0% of the time, Pallas kernels for 11%

profile of v2, /device:TPU:4, one launch (start us, length us, event | category | flops | bytes accessed | tf_op | source)
XLA Modules:
  0.0 95.3 jit_solution(11768115810546080699)
XLA Ops:
  0.6 3.1 %collective-permute-start.1 = (bf16[1024,256]{1,0:T(8,128)(2,1)}, bf16[1024,256]{1,0:T(8,128)(2,1)S(1)}, u32[]{:S(2)}, u32[]{:S(2)}) collective-permute-start(bf16[1024,256]{1,0:T(8,128)(2,1)} %refs_1_.1), channel_id=1, source_target_pairs={{0,2},{1,7},{2,4},{3,1},{4,6},{5,3},{6,0},{7,5},{8,10},{9,15},{10,... | collective-permute-start | bytes 1572872 | tf_op jit(solution)/shard_map/ppermute | solution.py:44
  3.7 2.7 %collective-permute-start.3 = (bf16[1024,256]{1,0:T(8,128)(2,1)}, bf16[1024,256]{1,0:T(8,128)(2,1)S(1)}, u32[]{:S(2)}, u32[]{:S(2)}) collective-permute-start(bf16[1024,256]{1,0:T(8,128)(2,1)} %refs_1_.1), channel_id=1, source_target_pairs={{0,6},{1,3},{2,0},{3,5},{4,2},{5,7},{6,4},{7,1},{8,14},{9,11},{10,... | collective-permute-start | bytes 1572872 | tf_op jit(solution)/shard_map/ppermute | solution.py:44
  6.5 10.0 %collective-permute-done.1.refs_2_.refs_3_ = bf16[1024,256]{1,0:T(8,128)(2,1)S(1)} collective-permute-done((bf16[1024,256]{1,0:T(8,128)(2,1)}, bf16[1024,256]{1,0:T(8,128)(2,1)S(1)}, u32[]{:S(2)}, u32[]{:S(2)}) %collective-permute-start.1) | collective-permute-done | bytes 524320 | tf_op jit(solution)/shard_map/ppermute | solution.py:44
  16.5 5.5 %collective-permute-start.5 = (bf16[1024,256]{1,0:T(8,128)(2,1)S(1)}, bf16[1024,256]{1,0:T(8,128)(2,1)S(1)}, u32[]{:S(2)}, u32[]{:S(2)}) collective-permute-start(bf16[1024,256]{1,0:T(8,128)(2,1)S(1)} %collective-permute-done.1.refs_2_.refs_3_), channel_id=1, source_target_pairs={{0,2},{1,7},{2,4},{3,1},{4,6},{5,3},{6,0},{7,5},{8,10},{9,15},{10,... | collective-permute-start | bytes 1572872 | tf_op jit(solution)/shard_map/ppermute | solution.py:44
  22.0 1.9 %collective-permute-start = (bf16[1024,256]{1,0:T(8,128)(2,1)}, bf16[1024,256]{1,0:T(8,128)(2,1)}, u32[]{:S(2)}, u32[]{:S(2)}) collective-permute-start(bf16[1024,256]{1,0:T(8,128)(2,1)} %refs_1_.1), channel_id=1, source_target_pairs={{0,1},{1,0},{2,3},{3,2},{4,5},{5,4},{6,7},{7,6},{8,9},{9,8},{10,11... | collective-permute-start | bytes 1572872 | tf_op jit(solution)/shard_map/ppermute | solution.py:38
  23.9 2.4 %collective-permute-start.2 = (bf16[1024,256]{1,0:T(8,128)(2,1)S(1)}, bf16[1024,256]{1,0:T(8,128)(2,1)}, u32[]{:S(2)}, u32[]{:S(2)}) collective-permute-start(bf16[1024,256]{1,0:T(8,128)(2,1)S(1)} %collective-permute-done.1.refs_2_.refs_3_), channel_id=1, source_target_pairs={{0,1},{1,0},{2,3},{3,2},{4,5},{5,4},{6,7},{7,6},{8,9},{9,8},{10,11... | collective-permute-start | bytes 1572872 | tf_op jit(solution)/shard_map/ppermute | solution.py:38
  26.3 0.0 collective-permute-done.3.refs_4_.refs_1_
  26.4 0.0 copy-start.1
  26.4 1.9 %collective-permute-start.4 = (bf16[1024,256]{1,0:T(8,128)(2,1)S(1)}, bf16[1024,256]{1,0:T(8,128)(2,1)S(1)}, u32[]{:S(2)}, u32[]{:S(2)}) collective-permute-start(bf16[1024,256]{1,0:T(8,128)(2,1)S(1)} %collective-permute-done.3.refs_4_.refs_1_), channel_id=1, source_target_pairs={{0,1},{1,0},{2,3},{3,2},{4,5},{5,4},{6,7},{7,6},{8,9},{9,8},{10,11... | collective-permute-start | bytes 1572872 | tf_op jit(solution)/shard_map/ppermute | solution.py:38
  28.3 0.9 collective-permute-done.5.refs_6_.refs_3_
  29.2 1.9 %collective-permute-start.6 = (bf16[1024,256]{1,0:T(8,128)(2,1)S(1)}, bf16[1024,256]{1,0:T(8,128)(2,1)S(1)}, u32[]{:S(2)}, u32[]{:S(2)}) collective-permute-start(bf16[1024,256]{1,0:T(8,128)(2,1)S(1)} %collective-permute-done.5.refs_6_.refs_3_), channel_id=1, source_target_pairs={{0,1},{1,0},{2,3},{3,2},{4,5},{5,4},{6,7},{7,6},{8,9},{9,8},{10,11... | collective-permute-start | bytes 1572872 | tf_op jit(solution)/shard_map/ppermute | solution.py:38
  31.1 0.0 copy-start
  31.1 1.2 %copy-done = bf16[1024,512]{1,0:T(8,128)(2,1)S(1)} copy-done((bf16[1024,512]{1,0:T(8,128)(2,1)S(1)}, bf16[1024,512]{1,0:T(8,128)(2,1)}, u32[]{:S(2)}) %copy-start) | copy-done | bytes 1048600
  32.3 1.1 %hidden.1.refs_0_ = bf16[512,1024]{1,0:T(8,128)(2,1)S(1)} custom-call(s32[1]{0:T(128)} %bitcast.at_ref.refs_0_, bf16[1024,512]{1,0:T(8,128)(2,1)S(1)} %copy-done), custom_call_target="tpu_custom_call" | custom-call | flops 536870912 | bytes 2097152 | tf_op jit(solution)/shard_map/hidden/pallas_call | solution.py:70
  33.4 0.0 collective-permute-done.refs_1_.refs_2_
  33.5 0.0 collective-permute-done.2.refs_3_.refs_4_
  33.5 0.0 copy-done.5
  33.5 2.5 %term.2.refs_5_ = bf16[512,2048]{1,0:T(8,128)(2,1)S(1)} custom-call(bf16[512,1024]{1,0:T(8,128)(2,1)S(1)} %hidden.1.refs_0_, bf16[1024,256]{1,0:T(8,128)(2,1)S(1)} %copy-done.5, bf16[1024,256]{1,0:T(8,128)(2,1)} %collective-permute-done.refs_1_.refs_2_, bf16[1024,256]{1,0:T(8,128)(2,1)S(1)} %collective-permute-done.1.refs_2_.refs_3_, ...), custom_call_target="tpu_custom_call" | custom-call | flops 1073741824 | bytes 4194304 | tf_op jit(solution)/shard_map/term/pallas_call | solution.py:101
  35.9 0.0 copy-done.6
  35.9 0.0 collective-permute-done.4.refs_5_.refs_2_
  36.0 0.0 copy-start.3
  36.0 0.0 collective-permute-done.6.refs_7_.refs_4_
  36.0 0.0 copy-done.1
  36.0 0.0 copy-done.2
  36.0 0.0 copy-start.4
  36.0 1.3 %term.3 = bf16[512,2048]{1,0:T(8,128)(2,1)S(1)} custom-call(bf16[512,1024]{1,0:T(8,128)(2,1)S(1)} %hidden.1.refs_0_, bf16[1024,256]{1,0:T(8,128)(2,1)S(1)} %collective-permute-done.3.refs_4_.refs_1_, bf16[1024,256]{1,0:T(8,128)(2,1)S(1)} %collective-permute-done.4.refs_5_.refs_2_, ...), custom_call_target="tpu_custom_call", output_to_operand_aliasing={{}: (5, {})} | custom-call | flops 1073741824 | bytes 4194304 | tf_op jit(solution)/shard_map/term/pallas_call | solution.py:101
  37.3 38.6 %all_to_all.18 = bf16[8,64,2048]{2,1,0:T(8,128)(2,1)S(1)} all-to-all(bf16[8,64,2048]{2,1,0:T(8,128)(2,1)S(1)} %bitcast.3), channel_id=1, replica_groups={{0,64,128,192,256,320,384,448},{8,72,136,200,264,328,392,456},{16,80,14..., dimensions={0} | all-to-all | bytes 4194304 | tf_op jit(solution)/shard_map/all_to_all | solution.py:33
  75.9 1.1 %reduce_sum.12 = bf16[64,2048]{1,0:T(8,128)(2,1)} reduce(bf16[8,64,2048]{2,1,0:T(8,128)(2,1)S(1)} %all_to_all.18, bf16[]{:T(256)} %constant.12.clone.1), dimensions={0}, to_apply=%region_0.0 | reduce | flops 917504 | bytes 2359298 | tf_op jit(solution)/shard_map/reduce_sum | solution.py:198
  77.0 7.1 %all-to-all-start.1 = ((bf16[8,8,2048]{2,1,0:T(8,128)(2,1)}), bf16[8,8,2048]{2,1,0:T(8,128)(2,1)S(1)}, u32[]{:S(2)}, u32[]{:S(2)}) async-start(bf16[8,8,2048]{2,1,0:T(8,128)(2,1)} %bitcast.2), calls=%async_computation.1 | async-start | bytes 524288 | tf_op jit(solution)/shard_map/all_to_all | solution.py:33
  84.1 6.9 %grad_pre.1 = bf16[1024,512]{1,0:T(8,128)(2,1)} custom-call(s32[1]{0:T(128)} %bitcast.at_ref.refs_0_, bf16[1024,512]{1,0:T(8,128)(2,1)} %pre_ref.3, bf16[512,2048]{1,0:T(8,128)(2,1)} %weight_ref.1, bf16[1024,256]{1,0:T(8,128)(2,1)} %refs_1_.1, bf16[1024,256]{1,0:T(8,128)(2,1)} %collective-permute-done.refs_1_.refs_2_, bf16[1024,256]{1,0:T(8,128)(2,1)} %copy-done.6, ...), custom_call_target="tpu_custom_call" | custom-call | flops 2147483648 | bytes 8388608 | tf_op jit(solution)/shard_map/grad_pre/pallas_call | solution.py:135
  91.0 3.6 %all-to-all-done.1.refs_1_ = bf16[8,8,2048]{2,1,0:T(8,128)(2,1)S(1)} async-done(((bf16[8,8,2048]{2,1,0:T(8,128)(2,1)}), bf16[8,8,2048]{2,1,0:T(8,128)(2,1)S(1)}, u32[]{:S(2)}, u32[]{:S(2)}) %all-to-all-start.1) | async-done | bytes 262176 | tf_op jit(solution)/shard_map/all_to_all | solution.py:33
  94.6 0.7 place.1
  (5 shorter events, 0.0 us)
Async XLA Ops:
  0.6 15.9 %collective-permute-start.1 = (bf16[1024,256]{1,0:T(8,128)(2,1)}, bf16[1024,256]{1,0:T(8,128)(2,1)S(1)}, u32[]{:S(2)}, u32[]{:S(2)}) collective-permute-start(bf16[1024,256]{1,0:T(8,128)(2,1)} %refs_1_.1), channel_id=1, source_target_pairs={{0,2},{1,7},{2,4},{3,1},{4,6},{5,3},{6,0},{7,5},{8,10},{9,15},{10,... | collective-permute-start | bytes 1572872 | tf_op jit(solution)/shard_map/ppermute | solution.py:44
  3.7 22.6 %collective-permute-start.3 = (bf16[1024,256]{1,0:T(8,128)(2,1)}, bf16[1024,256]{1,0:T(8,128)(2,1)S(1)}, u32[]{:S(2)}, u32[]{:S(2)}) collective-permute-start(bf16[1024,256]{1,0:T(8,128)(2,1)} %refs_1_.1), channel_id=1, source_target_pairs={{0,6},{1,3},{2,0},{3,5},{4,2},{5,7},{6,4},{7,1},{8,14},{9,11},{10,... | collective-permute-start | bytes 1572872 | tf_op jit(solution)/shard_map/ppermute | solution.py:44
  16.5 19.4 %copy-start.6 = (bf16[1024,256]{1,0:T(8,128)(2,1)}, bf16[1024,256]{1,0:T(8,128)(2,1)S(1)}, u32[]{:S(2)}) copy-start(bf16[1024,256]{1,0:T(8,128)(2,1)S(1)} %collective-permute-done.1.refs_2_.refs_3_) | copy-start | bytes 1572868
  16.5 12.7 %collective-permute-start.5 = (bf16[1024,256]{1,0:T(8,128)(2,1)S(1)}, bf16[1024,256]{1,0:T(8,128)(2,1)S(1)}, u32[]{:S(2)}, u32[]{:S(2)}) collective-permute-start(bf16[1024,256]{1,0:T(8,128)(2,1)S(1)} %collective-permute-done.1.refs_2_.refs_3_), channel_id=1, source_target_pairs={{0,2},{1,7},{2,4},{3,1},{4,6},{5,3},{6,0},{7,5},{8,10},{9,15},{10,... | collective-permute-start | bytes 1572872 | tf_op jit(solution)/shard_map/ppermute | solution.py:44
  22.0 11.4 %collective-permute-start = (bf16[1024,256]{1,0:T(8,128)(2,1)}, bf16[1024,256]{1,0:T(8,128)(2,1)}, u32[]{:S(2)}, u32[]{:S(2)}) collective-permute-start(bf16[1024,256]{1,0:T(8,128)(2,1)} %refs_1_.1), channel_id=1, source_target_pairs={{0,1},{1,0},{2,3},{3,2},{4,5},{5,4},{6,7},{7,6},{8,9},{9,8},{10,11... | collective-permute-start | bytes 1572872 | tf_op jit(solution)/shard_map/ppermute | solution.py:38
  23.9 9.5 %collective-permute-start.2 = (bf16[1024,256]{1,0:T(8,128)(2,1)S(1)}, bf16[1024,256]{1,0:T(8,128)(2,1)}, u32[]{:S(2)}, u32[]{:S(2)}) collective-permute-start(bf16[1024,256]{1,0:T(8,128)(2,1)S(1)} %collective-permute-done.1.refs_2_.refs_3_), channel_id=1, source_target_pairs={{0,1},{1,0},{2,3},{3,2},{4,5},{5,4},{6,7},{7,6},{8,9},{9,8},{10,11... | collective-permute-start | bytes 1572872 | tf_op jit(solution)/shard_map/ppermute | solution.py:38
  26.4 9.6 %copy-start.1 = (bf16[1024,256]{1,0:T(8,128)(2,1)}, bf16[1024,256]{1,0:T(8,128)(2,1)S(1)}, u32[]{:S(2)}) copy-start(bf16[1024,256]{1,0:T(8,128)(2,1)S(1)} %collective-permute-done.3.refs_4_.refs_1_) | copy-start | bytes 1572868
  26.4 9.6 %collective-permute-start.4 = (bf16[1024,256]{1,0:T(8,128)(2,1)S(1)}, bf16[1024,256]{1,0:T(8,128)(2,1)S(1)}, u32[]{:S(2)}, u32[]{:S(2)}) collective-permute-start(bf16[1024,256]{1,0:T(8,128)(2,1)S(1)} %collective-permute-done.3.refs_4_.refs_1_), channel_id=1, source_target_pairs={{0,1},{1,0},{2,3},{3,2},{4,5},{5,4},{6,7},{7,6},{8,9},{9,8},{10,11... | collective-permute-start | bytes 1572872 | tf_op jit(solution)/shard_map/ppermute | solution.py:38
  29.2 6.8 %copy-start.2 = (bf16[1024,256]{1,0:T(8,128)(2,1)}, bf16[1024,256]{1,0:T(8,128)(2,1)S(1)}, u32[]{:S(2)}) copy-start(bf16[1024,256]{1,0:T(8,128)(2,1)S(1)} %collective-permute-done.5.refs_6_.refs_3_) | copy-start | bytes 1572868
  29.2 6.8 %collective-permute-start.6 = (bf16[1024,256]{1,0:T(8,128)(2,1)S(1)}, bf16[1024,256]{1,0:T(8,128)(2,1)S(1)}, u32[]{:S(2)}, u32[]{:S(2)}) collective-permute-start(bf16[1024,256]{1,0:T(8,128)(2,1)S(1)} %collective-permute-done.5.refs_6_.refs_3_), channel_id=1, source_target_pairs={{0,1},{1,0},{2,3},{3,2},{4,5},{5,4},{6,7},{7,6},{8,9},{9,8},{10,11... | collective-permute-start | bytes 1572872 | tf_op jit(solution)/shard_map/ppermute | solution.py:38
  31.1 1.2 %copy-start = (bf16[1024,512]{1,0:T(8,128)(2,1)S(1)}, bf16[1024,512]{1,0:T(8,128)(2,1)}, u32[]{:S(2)}) copy-start(bf16[1024,512]{1,0:T(8,128)(2,1)} %pre_ref.3) | copy-start | bytes 3145732
  32.3 1.1 %copy-start.5 = (bf16[1024,256]{1,0:T(8,128)(2,1)S(1)}, bf16[1024,256]{1,0:T(8,128)(2,1)}, u32[]{:S(2)}) copy-start(bf16[1024,256]{1,0:T(8,128)(2,1)} %refs_1_.1) | copy-start | bytes 1572868
  36.0 1.3 %copy-start.3 = (bf16[1024,256]{1,0:T(8,128)(2,1)}, bf16[1024,256]{1,0:T(8,128)(2,1)S(1)}, u32[]{:S(2)}) copy-start(bf16[1024,256]{1,0:T(8,128)(2,1)S(1)} %collective-permute-done.4.refs_5_.refs_2_) | copy-start | bytes 1572868
  36.0 1.3 %copy-start.4 = (bf16[1024,256]{1,0:T(8,128)(2,1)}, bf16[1024,256]{1,0:T(8,128)(2,1)S(1)}, u32[]{:S(2)}) copy-start(bf16[1024,256]{1,0:T(8,128)(2,1)S(1)} %collective-permute-done.6.refs_7_.refs_4_) | copy-start | bytes 1572868
  77.0 17.6 %all-to-all-start.1 = ((bf16[8,8,2048]{2,1,0:T(8,128)(2,1)}), bf16[8,8,2048]{2,1,0:T(8,128)(2,1)S(1)}, u32[]{:S(2)}, u32[]{:S(2)}) async-start(bf16[8,8,2048]{2,1,0:T(8,128)(2,1)} %bitcast.2), calls=%async_computation.1 | async-start | bytes 524288 | tf_op jit(solution)/shard_map/all_to_all | solution.py:33

commit v3 on v2

--- a/solution.py
+++ b/solution.py
@@ -192,8 +192,10 @@
     pieces += (two, other_core(two), three, other_core(three))
 
     hidden = hidden_of(at, pre_act)
-    term = term_of(hidden, pieces[:4], 0, 8)
-    term = term_of(hidden, pieces[4:], 4, 8, term)
+    term = term_of(hidden, pieces[:2], 0, 8)
+    term = term_of(hidden, pieces[2:4], 2, 8, term)
+    term = term_of(hidden, pieces[4:6], 4, 8, term)
+    term = term_of(hidden, pieces[6:], 6, 8, term)
     got = swap(term, lines(size))
     joined = jnp.sum(got.astype(F32), axis=0).astype(BF16)
     got = swap(joined, other_lines(size))

time: 95.9 us -> 96.3 us (level)
    pallas_call x2 -> x4, Pallas kernels: 3.7 us -> 3.89 us  [term_of(): pl.pallas_call(lambda *refs: term_kernel(count, *refs), out_shape=jax.Sha...]
  transfers between devices with their start and end apart: 8 -> 8, of which waited for: 3 -> 3; matrix products, arithmetic and copies ran while one was open for 0% -> 0% of each run, Pallas kernels for 11% -> 12%
where the time goes in v3:
time: 96.3 us; the launch traced here: 95.7 us
  blocking collectives  38.6 us (40%)
  starting transfers between devices  26.6 us (28%)
  waiting for transfers between devices  14.5 us (15%)
  Pallas kernels  12.5 us (13%)
  local copies, waits for them, and re-layouts  1.49 us (2%)
  other arithmetic  1.13 us (1%)
    all_to_all x1, blocking collectives, swap(): lax.all_to_all(rows, GROUP, 0, 0, axis_index_groups=groups, tiled=True)  38.6 us
    ppermute x3, starting transfers between devices, along(): return lax.ppermute(x, COL, pairs)  11.3 us
    ppermute x3, waiting for transfers between devices, along(): return lax.ppermute(x, COL, pairs)  10.9 us
    ppermute x4, starting transfers between devices, other_core(): return lax.ppermute(x, 'tp', [(0, 1), (1, 0)])  8.16 us
    all_to_all x1, starting transfers between devices, swap(): lax.all_to_all(rows, GROUP, 0, 0, axis_index_groups=groups, tiled=True)  7.1 us
    pallas_call x1, Pallas kernels, grad_pre_of(): pl.pallas_call(grad_pre_kernel, out_shape=jax.ShapeDtypeStruct((tokens, u...  6.86 us
    pallas_call x4, Pallas kernels, term_of(): pl.pallas_call(lambda *refs: term_kernel(count, *refs), out_shape=jax.Sha...  3.89 us
    all_to_all x1, waiting for transfers between devices, swap(): lax.all_to_all(rows, GROUP, 0, 0, axis_index_groups=groups, tiled=True)  3.62 us
  transfers between devices with their start and end apart: 8, of which 3 were waited for; matrix products, arithmetic and copies ran while one was open for 0% of the time, Pallas kernels for 12%

profile of v3, /device:TPU:4, one launch (start us, length us, event | category | flops | bytes accessed | tf_op | source)
XLA Modules:
  0.0 95.7 jit_solution(17832847056838484456)
XLA Ops:
  0.6 3.1 %collective-permute-start.1 = (bf16[1024,256]{1,0:T(8,128)(2,1)}, bf16[1024,256]{1,0:T(8,128)(2,1)S(1)}, u32[]{:S(2)}, u32[]{:S(2)}) collective-permute-start(bf16[1024,256]{1,0:T(8,128)(2,1)} %refs_1_.1), channel_id=1, source_target_pairs={{0,2},{1,7},{2,4},{3,1},{4,6},{5,3},{6,0},{7,5},{8,10},{9,15},{10,... | collective-permute-start | bytes 1572872 | tf_op jit(solution)/shard_map/ppermute | solution.py:44
  3.7 2.7 %collective-permute-start.3 = (bf16[1024,256]{1,0:T(8,128)(2,1)}, bf16[1024,256]{1,0:T(8,128)(2,1)S(1)}, u32[]{:S(2)}, u32[]{:S(2)}) collective-permute-start(bf16[1024,256]{1,0:T(8,128)(2,1)} %refs_1_.1), channel_id=1, source_target_pairs={{0,6},{1,3},{2,0},{3,5},{4,2},{5,7},{6,4},{7,1},{8,14},{9,11},{10,... | collective-permute-start | bytes 1572872 | tf_op jit(solution)/shard_map/ppermute | solution.py:44
  6.5 10.0 %collective-permute-done.1.refs_2_.refs_1_ = bf16[1024,256]{1,0:T(8,128)(2,1)S(1)} collective-permute-done((bf16[1024,256]{1,0:T(8,128)(2,1)}, bf16[1024,256]{1,0:T(8,128)(2,1)S(1)}, u32[]{:S(2)}, u32[]{:S(2)}) %collective-permute-start.1) | collective-permute-done | bytes 524320 | tf_op jit(solution)/shard_map/ppermute | solution.py:44
  16.5 5.5 %collective-permute-start.5 = (bf16[1024,256]{1,0:T(8,128)(2,1)S(1)}, bf16[1024,256]{1,0:T(8,128)(2,1)S(1)}, u32[]{:S(2)}, u32[]{:S(2)}) collective-permute-start(bf16[1024,256]{1,0:T(8,128)(2,1)S(1)} %collective-permute-done.1.refs_2_.refs_1_), channel_id=1, source_target_pairs={{0,2},{1,7},{2,4},{3,1},{4,6},{5,3},{6,0},{7,5},{8,10},{9,15},{10,... | collective-permute-start | bytes 1572872 | tf_op jit(solution)/shard_map/ppermute | solution.py:44
  22.0 1.9 %collective-permute-start = (bf16[1024,256]{1,0:T(8,128)(2,1)}, bf16[1024,256]{1,0:T(8,128)(2,1)}, u32[]{:S(2)}, u32[]{:S(2)}) collective-permute-start(bf16[1024,256]{1,0:T(8,128)(2,1)} %refs_1_.1), channel_id=1, source_target_pairs={{0,1},{1,0},{2,3},{3,2},{4,5},{5,4},{6,7},{7,6},{8,9},{9,8},{10,11... | collective-permute-start | bytes 1572872 | tf_op jit(solution)/shard_map/ppermute | solution.py:38
  23.9 2.4 %collective-permute-start.2 = (bf16[1024,256]{1,0:T(8,128)(2,1)S(1)}, bf16[1024,256]{1,0:T(8,128)(2,1)S(1)}, u32[]{:S(2)}, u32[]{:S(2)}) collective-permute-start(bf16[1024,256]{1,0:T(8,128)(2,1)S(1)} %collective-permute-done.1.refs_2_.refs_1_), channel_id=1, source_target_pairs={{0,1},{1,0},{2,3},{3,2},{4,5},{5,4},{6,7},{7,6},{8,9},{9,8},{10,11... | collective-permute-start | bytes 1572872 | tf_op jit(solution)/shard_map/ppermute | solution.py:38
  26.3 0.0 collective-permute-done.3.refs_4_.refs_1_
  26.4 0.0 copy-start.2
  26.4 1.9 %collective-permute-start.4 = (bf16[1024,256]{1,0:T(8,128)(2,1)S(1)}, bf16[1024,256]{1,0:T(8,128)(2,1)S(1)}, u32[]{:S(2)}, u32[]{:S(2)}) collective-permute-start(bf16[1024,256]{1,0:T(8,128)(2,1)S(1)} %collective-permute-done.3.refs_4_.refs_1_), channel_id=1, source_target_pairs={{0,1},{1,0},{2,3},{3,2},{4,5},{5,4},{6,7},{7,6},{8,9},{9,8},{10,11... | collective-permute-start | bytes 1572872 | tf_op jit(solution)/shard_map/ppermute | solution.py:38
  28.3 0.9 collective-permute-done.5.refs_6_.refs_1_
  29.2 1.9 %collective-permute-start.6 = (bf16[1024,256]{1,0:T(8,128)(2,1)S(1)}, bf16[1024,256]{1,0:T(8,128)(2,1)S(1)}, u32[]{:S(2)}, u32[]{:S(2)}) collective-permute-start(bf16[1024,256]{1,0:T(8,128)(2,1)S(1)} %collective-permute-done.5.refs_6_.refs_1_), channel_id=1, source_target_pairs={{0,1},{1,0},{2,3},{3,2},{4,5},{5,4},{6,7},{7,6},{8,9},{9,8},{10,11... | collective-permute-start | bytes 1572872 | tf_op jit(solution)/shard_map/ppermute | solution.py:38
  31.1 0.0 copy-start
  31.1 1.2 %copy-done = bf16[1024,512]{1,0:T(8,128)(2,1)S(1)} copy-done((bf16[1024,512]{1,0:T(8,128)(2,1)S(1)}, bf16[1024,512]{1,0:T(8,128)(2,1)}, u32[]{:S(2)}) %copy-start) | copy-done | bytes 1048600
  32.3 1.1 %hidden.1.refs_0_ = bf16[512,1024]{1,0:T(8,128)(2,1)S(1)} custom-call(s32[1]{0:T(128)} %bitcast.at_ref.refs_0_, bf16[1024,512]{1,0:T(8,128)(2,1)S(1)} %copy-done), custom_call_target="tpu_custom_call" | custom-call | flops 536870912 | bytes 2097152 | tf_op jit(solution)/shard_map/hidden/pallas_call | solution.py:70
  33.4 0.0 collective-permute-done.refs_1_.refs_2_
  33.5 0.0 copy-done.7
  33.5 1.8 %term.4.refs_3_ = bf16[512,2048]{1,0:T(8,128)(2,1)S(1)} custom-call(bf16[512,1024]{1,0:T(8,128)(2,1)S(1)} %hidden.1.refs_0_, bf16[1024,256]{1,0:T(8,128)(2,1)S(1)} %copy-done.7, bf16[1024,256]{1,0:T(8,128)(2,1)} %collective-permute-done.refs_1_.refs_2_), custom_call_target="tpu_custom_call" | custom-call | flops 536870912 | bytes 2621440 | tf_op jit(solution)/shard_map/term/pallas_call | solution.py:101
  35.2 0.0 collective-permute-done.2.refs_3_.refs_2_
  35.3 0.7 term.5.refs_3_
  36.0 0.1 copy-done.4
  36.1 0.0 collective-permute-done.4.refs_5_.refs_2_
  36.1 0.7 term.6.refs_3_
  36.8 0.1 copy-done.5
  36.9 0.0 collective-permute-done.6.refs_7_.refs_2_
  36.9 0.7 term.7
  37.6 0.1 copy-done.6
  37.7 38.6 %all_to_all.18 = bf16[8,64,2048]{2,1,0:T(8,128)(2,1)S(1)} all-to-all(bf16[8,64,2048]{2,1,0:T(8,128)(2,1)S(1)} %bitcast.3), channel_id=1, replica_groups={{0,64,128,192,256,320,384,448},{8,72,136,200,264,328,392,456},{16,80,14..., dimensions={0} | all-to-all | bytes 4194304 | tf_op jit(solution)/shard_map/all_to_all | solution.py:33
  76.3 1.1 %reduce_sum.12 = bf16[64,2048]{1,0:T(8,128)(2,1)} reduce(bf16[8,64,2048]{2,1,0:T(8,128)(2,1)S(1)} %all_to_all.18, bf16[]{:T(256)} %constant.12.clone.1), dimensions={0}, to_apply=%region_0.0 | reduce | flops 917504 | bytes 2359298 | tf_op jit(solution)/shard_map/reduce_sum | solution.py:200
  77.4 7.1 %all-to-all-start.1 = ((bf16[8,8,2048]{2,1,0:T(8,128)(2,1)}), bf16[8,8,2048]{2,1,0:T(8,128)(2,1)S(1)}, u32[]{:S(2)}, u32[]{:S(2)}) async-start(bf16[8,8,2048]{2,1,0:T(8,128)(2,1)} %bitcast.2), calls=%async_computation.1 | async-start | bytes 524288 | tf_op jit(solution)/shard_map/all_to_all | solution.py:33
  84.5 6.9 %grad_pre.1 = bf16[1024,512]{1,0:T(8,128)(2,1)} custom-call(s32[1]{0:T(128)} %bitcast.at_ref.refs_0_, bf16[1024,512]{1,0:T(8,128)(2,1)} %pre_ref.3, bf16[512,2048]{1,0:T(8,128)(2,1)} %weight_ref.1, bf16[1024,256]{1,0:T(8,128)(2,1)} %refs_1_.1, bf16[1024,256]{1,0:T(8,128)(2,1)} %collective-permute-done.refs_1_.refs_2_, bf16[1024,256]{1,0:T(8,128)(2,1)} %copy-done.1, ...), custom_call_target="tpu_custom_call" | custom-call | flops 2147483648 | bytes 8388608 | tf_op jit(solution)/shard_map/grad_pre/pallas_call | solution.py:135
  91.4 3.6 %all-to-all-done.1.refs_1_ = bf16[8,8,2048]{2,1,0:T(8,128)(2,1)S(1)} async-done(((bf16[8,8,2048]{2,1,0:T(8,128)(2,1)}), bf16[8,8,2048]{2,1,0:T(8,128)(2,1)S(1)}, u32[]{:S(2)}, u32[]{:S(2)}) %all-to-all-start.1) | async-done | bytes 262176 | tf_op jit(solution)/shard_map/all_to_all | solution.py:33
  95.0 0.7 place.1
  (9 shorter events, 0.0 us)
Async XLA Ops:
  0.6 15.9 %collective-permute-start.1 = (bf16[1024,256]{1,0:T(8,128)(2,1)}, bf16[1024,256]{1,0:T(8,128)(2,1)S(1)}, u32[]{:S(2)}, u32[]{:S(2)}) collective-permute-start(bf16[1024,256]{1,0:T(8,128)(2,1)} %refs_1_.1), channel_id=1, source_target_pairs={{0,2},{1,7},{2,4},{3,1},{4,6},{5,3},{6,0},{7,5},{8,10},{9,15},{10,... | collective-permute-start | bytes 1572872 | tf_op jit(solution)/shard_map/ppermute | solution.py:44
  3.7 22.6 %collective-permute-start.3 = (bf16[1024,256]{1,0:T(8,128)(2,1)}, bf16[1024,256]{1,0:T(8,128)(2,1)S(1)}, u32[]{:S(2)}, u32[]{:S(2)}) collective-permute-start(bf16[1024,256]{1,0:T(8,128)(2,1)} %refs_1_.1), channel_id=1, source_target_pairs={{0,6},{1,3},{2,0},{3,5},{4,2},{5,7},{6,4},{7,1},{8,14},{9,11},{10,... | collective-permute-start | bytes 1572872 | tf_op jit(solution)/shard_map/ppermute | solution.py:44
  16.5 18.8 %copy-start.1 = (bf16[1024,256]{1,0:T(8,128)(2,1)}, bf16[1024,256]{1,0:T(8,128)(2,1)S(1)}, u32[]{:S(2)}) copy-start(bf16[1024,256]{1,0:T(8,128)(2,1)S(1)} %collective-permute-done.1.refs_2_.refs_1_) | copy-start | bytes 1572868
  16.5 12.7 %collective-permute-start.5 = (bf16[1024,256]{1,0:T(8,128)(2,1)S(1)}, bf16[1024,256]{1,0:T(8,128)(2,1)S(1)}, u32[]{:S(2)}, u32[]{:S(2)}) collective-permute-start(bf16[1024,256]{1,0:T(8,128)(2,1)S(1)} %collective-permute-done.1.refs_2_.refs_1_), channel_id=1, source_target_pairs={{0,2},{1,7},{2,4},{3,1},{4,6},{5,3},{6,0},{7,5},{8,10},{9,15},{10,... | collective-permute-start | bytes 1572872 | tf_op jit(solution)/shard_map/ppermute | solution.py:44
  22.0 11.4 %collective-permute-start = (bf16[1024,256]{1,0:T(8,128)(2,1)}, bf16[1024,256]{1,0:T(8,128)(2,1)}, u32[]{:S(2)}, u32[]{:S(2)}) collective-permute-start(bf16[1024,256]{1,0:T(8,128)(2,1)} %refs_1_.1), channel_id=1, source_target_pairs={{0,1},{1,0},{2,3},{3,2},{4,5},{5,4},{6,7},{7,6},{8,9},{9,8},{10,11... | collective-permute-start | bytes 1572872 | tf_op jit(solution)/shard_map/ppermute | solution.py:38
  23.9 11.3 %collective-permute-start.2 = (bf16[1024,256]{1,0:T(8,128)(2,1)S(1)}, bf16[1024,256]{1,0:T(8,128)(2,1)S(1)}, u32[]{:S(2)}, u32[]{:S(2)}) collective-permute-start(bf16[1024,256]{1,0:T(8,128)(2,1)S(1)} %collective-permute-done.1.refs_2_.refs_1_), channel_id=1, source_target_pairs={{0,1},{1,0},{2,3},{3,2},{4,5},{5,4},{6,7},{7,6},{8,9},{9,8},{10,11... | collective-permute-start | bytes 1572872 | tf_op jit(solution)/shard_map/ppermute | solution.py:38
  26.4 9.7 %copy-start.2 = (bf16[1024,256]{1,0:T(8,128)(2,1)}, bf16[1024,256]{1,0:T(8,128)(2,1)S(1)}, u32[]{:S(2)}) copy-start(bf16[1024,256]{1,0:T(8,128)(2,1)S(1)} %collective-permute-done.3.refs_4_.refs_1_) | copy-start | bytes 1572868
  26.4 9.7 %collective-permute-start.4 = (bf16[1024,256]{1,0:T(8,128)(2,1)S(1)}, bf16[1024,256]{1,0:T(8,128)(2,1)S(1)}, u32[]{:S(2)}, u32[]{:S(2)}) collective-permute-start(bf16[1024,256]{1,0:T(8,128)(2,1)S(1)} %collective-permute-done.3.refs_4_.refs_1_), channel_id=1, source_target_pairs={{0,1},{1,0},{2,3},{3,2},{4,5},{5,4},{6,7},{7,6},{8,9},{9,8},{10,11... | collective-permute-start | bytes 1572872 | tf_op jit(solution)/shard_map/ppermute | solution.py:38
  29.2 7.7 %copy-start.3 = (bf16[1024,256]{1,0:T(8,128)(2,1)}, bf16[1024,256]{1,0:T(8,128)(2,1)S(1)}, u32[]{:S(2)}) copy-start(bf16[1024,256]{1,0:T(8,128)(2,1)S(1)} %collective-permute-done.5.refs_6_.refs_1_) | copy-start | bytes 1572868
  29.2 7.7 %collective-permute-start.6 = (bf16[1024,256]{1,0:T(8,128)(2,1)S(1)}, bf16[1024,256]{1,0:T(8,128)(2,1)S(1)}, u32[]{:S(2)}, u32[]{:S(2)}) collective-permute-start(bf16[1024,256]{1,0:T(8,128)(2,1)S(1)} %collective-permute-done.5.refs_6_.refs_1_), channel_id=1, source_target_pairs={{0,1},{1,0},{2,3},{3,2},{4,5},{5,4},{6,7},{7,6},{8,9},{9,8},{10,11... | collective-permute-start | bytes 1572872 | tf_op jit(solution)/shard_map/ppermute | solution.py:38
  31.1 1.2 %copy-start = (bf16[1024,512]{1,0:T(8,128)(2,1)S(1)}, bf16[1024,512]{1,0:T(8,128)(2,1)}, u32[]{:S(2)}) copy-start(bf16[1024,512]{1,0:T(8,128)(2,1)} %pre_ref.3) | copy-start | bytes 3145732
  32.3 1.1 %copy-start.7 = (bf16[1024,256]{1,0:T(8,128)(2,1)S(1)}, bf16[1024,256]{1,0:T(8,128)(2,1)}, u32[]{:S(2)}) copy-start(bf16[1024,256]{1,0:T(8,128)(2,1)} %refs_1_.1) | copy-start | bytes 1572868
  35.3 0.8 copy-start.4
  36.1 0.8 copy-start.5
  36.9 0.8 copy-start.6
  77.4 17.6 %all-to-all-start.1 = ((bf16[8,8,2048]{2,1,0:T(8,128)(2,1)}), bf16[8,8,2048]{2,1,0:T(8,128)(2,1)S(1)}, u32[]{:S(2)}, u32[]{:S(2)}) async-start(bf16[8,8,2048]{2,1,0:T(8,128)(2,1)} %bitcast.2), calls=%async_computation.1 | async-start | bytes 524288 | tf_op jit(solution)/shard_map/all_to_all | solution.py:33
